TPU v7x, 32 devices: a whole 2x2x4 slice. The times are simulated.
32 devices in a mesh: ep: 4 (over z), tp: 8 (over y, x, core).
Axes of the slice: x: 2, y: 2, z: 4, core: 2. Of those that a mesh axis runs over, the one named last changes fastest.
Arguments:
- hidden: bfloat16 [64, 4096], P('ep', 'tp'), may hold values from -6 to 6
- norm_gain: float32 [4096], replicated, may hold values from 0.1 to 1.9
- routes: int32 [64, 4], P('ep'), may hold values from 0 to 7, all different within a row; in each aligned block of 16 rows (0 to 15, 16 to 31, ...) at most 13 rows name the same one
- route_weights: float32 [64, 4], P('ep'), may hold values from 0.1 to 1
- gate_weight: bfloat16 [8, 1024, 4096], P('ep', 'tp'), may hold values from -0.09375 to 0.09375
- up_weight: bfloat16 [8, 1024, 4096], P('ep', 'tp'), may hold values from -0.09375 to 0.09375
- down_weight: bfloat16 [8, 1024, 4096], P('ep', 'tp'), may hold values from -0.25 to 0.25
- shared_gate: bfloat16 [1024, 4096], P('tp'), may hold values from -0.09375 to 0.09375
- shared_up: bfloat16 [1024, 4096], P('tp'), may hold values from -0.09375 to 0.09375
- shared_down: bfloat16 [1024, 4096], P('tp'), may hold values from -0.25 to 0.25
Outputs:
- mixed: bfloat16 [64, 4096], P('ep', 'tp')
Inputs may be any that keep to these rules, and one draw needn't show every extreme that they name: `routes`: each row names 4 different experts; among the rows of one index of ep (aligned blocks of 16 rows) no expert is named more than 13 times, a bound that some block reaches.
All inputs are finite; a program needn't handle non-finite values.
Results may differ from a plain program's by a relative error of at most 0.017.
Values may be sent and summed in bfloat16 or wider, within the bound.
A program may use at most 64 MiB of HBM per device.

v0:
```python
import jax
import jax.numpy as jnp
from jax import lax
from jax.sharding import PartitionSpec as P

norm_eps = 1e-06


def norm_rows(gathered, norm_gain):
    values = gathered.astype(jnp.float32)
    inv_scale = lax.rsqrt(jnp.mean(values * values, axis=-1, keepdims=True) + norm_eps)
    return (values * inv_scale * norm_gain).astype(jnp.bfloat16)


def slot_table(routes, expert_count, capacity):
    onehot = (
        routes[:, :, None] == jnp.arange(expert_count, dtype=jnp.int32)[None, None, :]
    ).astype(jnp.int32)
    used_mask = jnp.sum(onehot, axis=1)
    before = jnp.cumsum(used_mask, axis=0) - used_mask
    slot_rank = jnp.sum(onehot * before[:, None, :], axis=2)
    return routes * capacity + slot_rank


def per_device(
    hidden,
    norm_gain,
    routes,
    route_weights,
    gate_weight,
    up_weight,
    down_weight,
    shared_gate,
    shared_up,
    shared_down,
):
    width_group = lax.axis_size("tp")
    down_local = lax.all_to_all(down_weight, "tp", split_axis=2, concat_axis=1, tiled=True)
    gathered = lax.all_gather(hidden, "tp", axis=1, tiled=True)
    normed = norm_rows(gathered, norm_gain)
    tok_rows, top_count = routes.shape
    local_experts = gate_weight.shape[0]
    groups = lax.axis_size("ep")
    experts = local_experts * groups
    capacity = min(tok_rows, 3 * tok_rows * top_count // (2 * experts) + 1)
    full_width = gathered.shape[1]
    slot_ids = slot_table(routes, experts, capacity)
    slot_range = jnp.arange(experts * capacity, dtype=jnp.int32)
    matches = slot_ids[:, :, None] == slot_range[None, None, :]
    combine = jnp.sum(jnp.where(matches, route_weights[:, :, None], 0.0), axis=1)
    select = jnp.sum(
        (slot_range[:, None, None] == slot_ids[None, :, :]).astype(jnp.bfloat16), axis=2
    )
    packed = jnp.dot(select, normed, preferred_element_type=jnp.float32).astype(jnp.bfloat16)
    packed = packed.reshape(groups, local_experts, capacity, full_width)
    arrived = lax.all_to_all(packed, "ep", split_axis=0, concat_axis=0, tiled=True)
    gate_vals = jnp.einsum(
        "secd,efd->secf", arrived, gate_weight, preferred_element_type=jnp.float32
    )
    up_vals = jnp.einsum("secd,efd->secf", arrived, up_weight, preferred_element_type=jnp.float32)
    inner_vals = (jax.nn.silu(gate_vals) * up_vals).astype(jnp.bfloat16)
    dims = (((1,), (1,)), ((), ()))
    shared_gates = lax.dot_general(normed, shared_gate, dims, preferred_element_type=jnp.float32)
    shared_ups = lax.dot_general(normed, shared_up, dims, preferred_element_type=jnp.float32)
    shared_inner = (jax.nn.silu(shared_gates) * shared_ups).astype(jnp.bfloat16)
    shared_part = jnp.dot(shared_inner, shared_down, preferred_element_type=jnp.float32).astype(
        jnp.bfloat16
    )
    inner_whole = lax.all_gather(inner_vals, "tp", axis=3, tiled=True)
    slots, _, cap_rows, hidden_units = inner_whole.shape
    block_units = hidden_units // width_group
    inner_blocks = inner_whole.reshape(slots, local_experts, cap_rows, width_group, block_units)
    down_blocks = down_local.reshape(local_experts, width_group, block_units, down_local.shape[2])
    block_sums = jnp.einsum(
        "secpf,epfd->secpd", inner_blocks, down_blocks, preferred_element_type=jnp.float32
    ).astype(jnp.bfloat16)
    answers = jnp.sum(block_sums.astype(jnp.float32), axis=3).astype(jnp.bfloat16)
    shared_sum = lax.psum_scatter(shared_part, "tp", scatter_dimension=1, tiled=True).astype(
        jnp.float32
    )
    returned = lax.all_to_all(answers, "ep", split_axis=0, concat_axis=0, tiled=True)
    flat_rows = returned.reshape(-1, returned.shape[3]).astype(jnp.float32)
    routed = jnp.dot(combine, flat_rows, precision=lax.Precision.HIGHEST)
    return (routed + shared_sum).astype(jnp.bfloat16)


def solution(mesh):
    in_specs = (
        P("ep", "tp"),
        P(),
        P("ep", None),
        P("ep", None),
        P("ep", "tp", None),
        P("ep", "tp", None),
        P("ep", "tp", None),
        P("tp", None),
        P("tp", None),
        P("tp", None),
    )
    out_specs = P("ep", "tp")
    return jax.shard_map(
        per_device, mesh=mesh, in_specs=in_specs, out_specs=out_specs, check_vma=False
    )
```

profile of v0, /device:TPU:0, one launch (start us, length us, event | category | flops | bytes accessed | tf_op | source)
XLA Modules:
  0.0 113.9 jit_solution(8584589679115222297)
XLA Ops:
  6.5 0.8 convert_reduce_fusion
  7.6 0.7 select_reduce_fusion.1
  8.3 0.7 multiply_add_fusion
  9.0 10.9 %all_gather.6 = bf16[16,4096]{1,0:T(8,128)(2,1)S(1)} all-gather(bf16[16,512]{1,0:T(8,128)(2,1)} %param.10), channel_id=1, replica_groups=mesh['ep'=4,'tp'=8] {'tp'}, dimensions={1}, use_global_device_ids=true | all-gather | bytes 147456 | tf_op jit(solution)/shard_map/all_gather | solution.py:39
  20.1 2.1 %convolution_convert_fusion = bf16[104,4096]{1,0:T(8,128)(2,1)} fusion(bf16[104,16]{0,1:T(8,128)(2,1)S(1)} %fusion.33, bf16[16,4096]{1,0:T(8,128)(2,1)S(1)} %all_gather.6, f32[4096]{0:T(1024)} %param.11, f32[16]{0:T(128)S(1)} %add_rsqrt_fusion), kind=kOutput, calls=%fused_computation | convolution fusion | flops 14319616 | bytes 1002816 | tf_op jit(solution)/shard_map/dot_general | solution.py:54
  22.2 1.4 %reshape.33 = bf16[4,2,13,4096]{3,2,1,0:T(8,128)(2,1)S(1)} reshape(bf16[104,4096]{1,0:T(8,128)(2,1)} %convolution_convert_fusion) | data formatting | bytes 1703936 | tf_op jit(solution)/shard_map/reshape | solution.py:55
  23.6 1.8 %copy.43 = bf16[4,2,13,4096]{3,1,2,0:T(2,128)(2,1)} copy(bf16[4,2,13,4096]{3,2,1,0:T(8,128)(2,1)S(1)} %reshape.33) | data formatting | bytes 1703936 | tf_op jit(solution)/shard_map/reshape | solution.py:55
  25.4 4.9 %all-to-all-start = ((bf16[4,2,13,4096]{3,1,2,0:T(2,128)(2,1)}), bf16[4,2,13,4096]{3,1,2,0:T(2,128)(2,1)S(1)}, u32[]{:S(2)}, u32[]{:S(2)}) async-start(bf16[4,2,13,4096]{3,1,2,0:T(2,128)(2,1)} %copy.43), calls=%async_computation | async-start | bytes 1703936 | tf_op jit(solution)/shard_map/all_to_all | solution.py:56
  30.3 6.2 %copy.47 = bf16[2,128,4096]{1,0,2:T(2,128)(2,1)} copy(bf16[2,128,4096]{2,1,0:T(8,128)(2,1)} %param.16) | data formatting | bytes 4194304 | tf_op args[6]
  36.5 15.8 %all-to-all-done = bf16[4,2,13,4096]{3,1,2,0:T(2,128)(2,1)S(1)} async-done(((bf16[4,2,13,4096]{3,1,2,0:T(2,128)(2,1)}), bf16[4,2,13,4096]{3,1,2,0:T(2,128)(2,1)S(1)}, u32[]{:S(2)}, u32[]{:S(2)}) %all-to-all-start) | async-done | bytes 852000 | tf_op jit(solution)/shard_map/all_to_all | solution.py:56
  52.3 4.3 %all-to-all-start.1 = ((bf16[2,128,4096]{1,0,2:T(2,128)(2,1)}), bf16[2,128,4096]{1,0,2:T(2,128)(2,1)}, u32[]{:S(2)}, u32[]{:S(2)}) async-start(bf16[2,128,4096]{1,0,2:T(2,128)(2,1)} %copy.47), calls=%async_computation.1 | async-start | bytes 4194304 | tf_op jit(solution)/shard_map/all_to_all | solution.py:38
  56.7 1.6 %fusion.43 = f32[16,128]{1,0:T(8,128)S(1)} fusion(bf16[128,4096]{1,0:T(8,128)(2,1)} %param.17, bf16[16,4096]{1,0:T(8,128)(2,1)S(1)} %all_gather.6, f32[4096]{0:T(1024)S(1)} %copy-done.2, f32[16]{0:T(128)S(1)} %add_rsqrt_fusion), kind=kOutput, calls=%fused_computation.43 | convolution fusion | flops 17039360 | bytes 1204288 | tf_op jit(solution)/shard_map/dot_general | solution.py:63
  58.4 3.1 %convolution_convert_fusion.1 = bf16[16,4096]{1,0:T(8,128)(2,1)} fusion(bf16[128,4096]{1,0:T(8,128)(2,1)} %param.19, bf16[128,4096]{1,0:T(8,128)(2,1)} %param.18, f32[16,128]{1,0:T(8,128)S(1)} %fusion.43, bf16[16,4096]{1,0:T(8,128)(2,1)S(1)} %all_gather.6, f32[4096]{0:T(1024)S(1)} %copy-done.2, f32[16]{0:T(128)S(1)} %add_rsqrt_fusion), kind=kOutput, calls=%fused_computation.1 | convolution fusion | flops 33894400 | bytes 2383936 | tf_op jit(solution)/shard_map/dot_general | solution.py:66
  61.6 0.8 fusion.12
  62.4 0.7 copy-done.1
  63.1 0.9 fusion.21
  64.0 22.9 %all_gather.7 = bf16[4,2,13,1024]{3,2,0,1:T(8,128)(2,1)S(1)} all-gather(bf16[4,2,13,128]{3,2,0,1:T(8,128)(2,1)S(1)} %fusion.21), channel_id=1, replica_groups=mesh['ep'=4,'tp'=8] {'tp'}, dimensions={3}, use_global_device_ids=true | all-gather | bytes 239616 | tf_op jit(solution)/shard_map/all_gather | solution.py:69
  86.9 0.2 reshape.39
  87.1 6.2 %copy.49 = bf16[2,128,8,512]{3,1,2,0:T(8,128)(2,1)} copy(bf16[2,128,8,512]{1,0,3,2:T(2,128)(2,1)} %bitcast.6) | data formatting | bytes 4194304 | tf_op jit(solution)/shard_map/all_to_all | solution.py:38
  93.2 2.1 %fusion.9 = bf16[2,4,13,512]{3,2,1,0:T(8,128)(2,1)S(1)} fusion(bf16[2,128,8,512]{3,1,2,0:T(8,128)(2,1)} %copy.49, bf16[4,2,13,8,128]{4,3,2,0,1:T(8,128)(2,1)S(1)} %reshape.39), kind=kOutput, calls=%fused_computation.9 | convolution fusion | flops 109850624 | bytes 2416640 | tf_op jit(solution)/shard_map/secpf,epfd->secpd/dot_general | solution.py:74
  95.3 0.8 copy.51
  96.1 3.3 %all-to-all-start.2 = ((bf16[4,2,13,512]{3,1,2,0:T(2,128)(2,1)}), bf16[4,2,13,512]{3,1,2,0:T(2,128)(2,1)S(1)}, u32[]{:S(2)}, u32[]{:S(2)}) async-start(bf16[4,2,13,512]{3,1,2,0:T(2,128)(2,1)} %copy.51), calls=%async_computation.2 | async-start | bytes 212992 | tf_op jit(solution)/shard_map/all_to_all | solution.py:81
  99.5 6.0 %all-to-all-done.2 = bf16[4,2,13,512]{3,1,2,0:T(2,128)(2,1)S(1)} async-done(((bf16[4,2,13,512]{3,1,2,0:T(2,128)(2,1)}), bf16[4,2,13,512]{3,1,2,0:T(2,128)(2,1)S(1)}, u32[]{:S(2)}, u32[]{:S(2)}) %all-to-all-start.2) | async-done | bytes 106528 | tf_op jit(solution)/shard_map/all_to_all | solution.py:81
  105.6 1.5 %fusion.24 = bf16[16,512]{1,0:T(8,128)(2,1)} fusion(f32[16,104]{1,0:T(8,128)S(1)} %select_reduce_fusion, bf16[104,512]{1,0:T(8,128)(2,1)S(1)} %reshape.35, bf16[16,512]{1,0:T(8,128)(2,1)} %reduce-scatter.2.cloned.1.call-done), kind=kOutput, calls=%fused_computation.15 | convolution fusion | flops 10248192 | bytes 145920 | tf_op jit(solution)/shard_map/dot_general | solution.py:83
  (21 shorter events, 0.7 us)
Async XLA Ops:
  6.5 55.0 %copy-start = (bf16[2,128,4096]{2,1,0:T(8,128)(2,1)S(1)}, bf16[2,128,4096]{2,1,0:T(8,128)(2,1)}, u32[]{:S(2)}) copy-start(bf16[2,128,4096]{2,1,0:T(8,128)(2,1)} %param.14) | copy-start | bytes 6291460
  25.4 26.9 %all-to-all-start = ((bf16[4,2,13,4096]{3,1,2,0:T(2,128)(2,1)}), bf16[4,2,13,4096]{3,1,2,0:T(2,128)(2,1)S(1)}, u32[]{:S(2)}, u32[]{:S(2)}) async-start(bf16[4,2,13,4096]{3,1,2,0:T(2,128)(2,1)} %copy.43), calls=%async_computation | async-start | bytes 1703936 | tf_op jit(solution)/shard_map/all_to_all | solution.py:56
  36.5 20.2 %copy-start.2 = (f32[4096]{0:T(1024)S(1)}, f32[4096]{0:T(1024)}, u32[]{:S(2)}) copy-start(f32[4096]{0:T(1024)} %param.11) | copy-start | bytes 49156
  52.3 34.8 %all-to-all-start.1 = ((bf16[2,128,4096]{1,0,2:T(2,128)(2,1)}), bf16[2,128,4096]{1,0,2:T(2,128)(2,1)}, u32[]{:S(2)}, u32[]{:S(2)}) async-start(bf16[2,128,4096]{1,0,2:T(2,128)(2,1)} %copy.47), calls=%async_computation.1 | async-start | bytes 4194304 | tf_op jit(solution)/shard_map/all_to_all | solution.py:38
  56.7 48.9 %reduce-scatter.2.cloned.1.call-start = ((), (), s32[]{:S(2)}) async-start(), calls=%async_computation.4 | async-start | bytes 147456 | tf_op jit(solution)/shard_map/reduce_scatter | solution.py:78
  61.6 1.6 %copy-start.1 = (bf16[2,128,4096]{2,1,0:T(8,128)(2,1)S(1)}, bf16[2,128,4096]{2,1,0:T(8,128)(2,1)}, u32[]{:S(2)}) copy-start(bf16[2,128,4096]{2,1,0:T(8,128)(2,1)} %param.15) | copy-start | bytes 6291460
  93.2 6.1 %copy-start.3 = (f32[16,4]{0,1:T(4,128)S(1)}, f32[16,4]{0,1:T(4,128)}, u32[]{:S(2)}) copy-start(f32[16,4]{0,1:T(4,128)} %param.13) | copy-start | bytes 772
  96.1 9.4 %all-to-all-start.2 = ((bf16[4,2,13,512]{3,1,2,0:T(2,128)(2,1)}), bf16[4,2,13,512]{3,1,2,0:T(2,128)(2,1)S(1)}, u32[]{:S(2)}, u32[]{:S(2)}) async-start(bf16[4,2,13,512]{3,1,2,0:T(2,128)(2,1)} %copy.51), calls=%async_computation.2 | async-start | bytes 212992 | tf_op jit(solution)/shard_map/all_to_all | solution.py:81
Sparse Core Ops, SparseCore 0:
  61.7 33.0 reduce-scatter.1
where the time goes:
time: 115 us; the launch traced here: 114 us
  blocking collectives  33.8 us (29%)
  waiting for transfers between devices  21.8 us (19%)
  local copies, waits for them, and re-layouts  17.5 us (15%)
  between operations  13.5 us (12%)
  starting transfers between devices  12.6 us (11%)
  matrix products  12.1 us (11%)
  other arithmetic  2.59 us (2%)
    all_gather x1, blocking collectives, per_device(): inner_whole = lax.all_gather(inner_vals, 'tp', axis=3, tiled=True)  22.9 us
    all_to_all x1, waiting for transfers between devices, per_device(): lax.all_to_all(packed, 'ep', split_axis=0, concat_axis=0, tiled=True)  15.8 us
    all_gather x1, blocking collectives, per_device(): gathered = lax.all_gather(hidden, 'tp', axis=1, tiled=True)  10.9 us
    unnamed x9, local copies, waits for them, and re-layouts  6.96 us
    all_to_all x1, local copies, waits for them, and re-layouts, per_device(): lax.all_to_all(down_weight, 'tp', split_axis=2, concat_axis=1, tiled=True)  6.15 us
    all_to_all x1, waiting for transfers between devices, per_device(): lax.all_to_all(answers, 'ep', split_axis=0, concat_axis=0, tiled=True)  5.96 us
    all_to_all x1, starting transfers between devices, per_device(): lax.all_to_all(packed, 'ep', split_axis=0, concat_axis=0, tiled=True)  4.87 us
    all_to_all x1, starting transfers between devices, per_device(): lax.all_to_all(down_weight, 'tp', split_axis=2, concat_axis=1, tiled=True)  4.34 us
  transfers between devices with their start and end apart: 4, of which 2 were waited for; matrix products, arithmetic and copies ran while one was open for 19% of the time, Pallas kernels for 0%

commit v1 on v0

--- a/solution.py
+++ b/solution.py
@@ -36,7 +36,12 @@
 ):
     width_group = lax.axis_size("tp")
     down_local = lax.all_to_all(down_weight, "tp", split_axis=2, concat_axis=1, tiled=True)
-    gathered = lax.all_gather(hidden, "tp", axis=1, tiled=True)
+    ring = [hidden]
+    for hop in range(7):
+        ring.append(lax.ppermute(ring[-1], "tp", [(dev, (dev + 1) % 8) for dev in range(8)]))
+    gathered = jnp.roll(
+        jnp.concatenate(ring[::-1], axis=1), (lax.axis_index("tp") + 1) * ring[0].shape[1], axis=1
+    )
     normed = norm_rows(gathered, norm_gain)
     tok_rows, top_count = routes.shape
     local_experts = gate_weight.shape[0]

time: 115 us -> 130 us (1.13)
  waiting for transfers between devices: 21.8 us -> 45.1 us
  blocking collectives: 33.8 us -> 22.9 us
  local copies, waits for them, and re-layouts: 17.5 us -> 19 us
    ppermute x0 -> x7, waiting for transfers between devices: none -> 26.5 us  [per_device(): lax.ppermute(ring[-1], 'tp', [(dev, (dev + 1) % 8) for dev in range(8)])]
    all_gather x1 -> x0, blocking collectives: 10.9 us -> none  [per_device(): gathered = lax.all_gather(hidden, 'tp', axis=1, tiled=True)]
    all_to_all x1, waiting for transfers between devices: 15.8 us -> 12.6 us  [per_device(): lax.all_to_all(packed, 'ep', split_axis=0, concat_axis=0, tiled=True)]
    unnamed x9 -> x24, local copies, waits for them, and re-layouts: 6.96 us -> 7.72 us
  transfers between devices with their start and end apart: 4 -> 11, of which waited for: 2 -> 9; matrix products, arithmetic and copies ran while one was open for 19% -> 19% of each run, Pallas kernels for 0% -> 0%
where the time goes in v1:
time: 130 us; the launch traced here: 129 us
  waiting for transfers between devices  45.1 us (35%)
  blocking collectives  22.9 us (18%)
  local copies, waits for them, and re-layouts  19 us (15%)
  starting transfers between devices  13.8 us (11%)
  between operations  13.6 us (10%)
  matrix products  12.1 us (9%)
  other arithmetic  2.43 us (2%)
    ppermute x7, waiting for transfers between devices, per_device(): lax.ppermute(ring[-1], 'tp', [(dev, (dev + 1) % 8) for dev in range(8)])  26.5 us
    all_gather x1, blocking collectives, per_device(): inner_whole = lax.all_gather(inner_vals, 'tp', axis=3, tiled=True)  22.9 us
    all_to_all x1, waiting for transfers between devices, per_device(): lax.all_to_all(packed, 'ep', split_axis=0, concat_axis=0, tiled=True)  12.6 us
    unnamed x24, local copies, waits for them, and re-layouts  7.72 us
    all_to_all x1, local copies, waits for them, and re-layouts, per_device(): lax.all_to_all(down_weight, 'tp', split_axis=2, concat_axis=1, tiled=True)  6.15 us
    all_to_all x1, waiting for transfers between devices, per_device(): lax.all_to_all(answers, 'ep', split_axis=0, concat_axis=0, tiled=True)  5.96 us
    all_to_all x1, starting transfers between devices, per_device(): lax.all_to_all(packed, 'ep', split_axis=0, concat_axis=0, tiled=True)  5.63 us
    all_to_all x1, starting transfers between devices, per_device(): lax.all_to_all(down_weight, 'tp', split_axis=2, concat_axis=1, tiled=True)  4.34 us
  transfers between devices with their start and end apart: 11, of which 9 were waited for; matrix products, arithmetic and copies ran while one was open for 19% of the time, Pallas kernels for 0%

profile of v1, /device:TPU:0, one launch (start us, length us, event | category | flops | bytes accessed | tf_op | source)
XLA Modules:
  0.0 128.9 jit_solution(14661916100457475905)
XLA Ops:
  7.0 4.5 %collective-permute-done = bf16[16,512]{1,0:T(8,128)(2,1)S(1)} collective-permute-done((bf16[16,512]{1,0:T(8,128)(2,1)}, bf16[16,512]{1,0:T(8,128)(2,1)S(1)}, u32[]{:S(2)}, u32[]{:S(2)}) %collective-permute-start) | collective-permute-done | bytes 16416 | tf_op jit(solution)/shard_map/ppermute | solution.py:41
  11.5 4.1 %collective-permute-done.1 = bf16[16,512]{1,0:T(8,128)(2,1)S(1)} collective-permute-done((bf16[16,512]{1,0:T(8,128)(2,1)S(1)}, bf16[16,512]{1,0:T(8,128)(2,1)S(1)}, u32[]{:S(2)}, u32[]{:S(2)}) %collective-permute-start.1) | collective-permute-done | bytes 16416 | tf_op jit(solution)/shard_map/ppermute | solution.py:41
  15.6 4.1 %collective-permute-done.2 = bf16[16,512]{1,0:T(8,128)(2,1)S(1)} collective-permute-done((bf16[16,512]{1,0:T(8,128)(2,1)S(1)}, bf16[16,512]{1,0:T(8,128)(2,1)S(1)}, u32[]{:S(2)}, u32[]{:S(2)}) %collective-permute-start.2) | collective-permute-done | bytes 16416 | tf_op jit(solution)/shard_map/ppermute | solution.py:41
  20.5 3.2 %collective-permute-done.3 = bf16[16,512]{1,0:T(8,128)(2,1)S(1)} collective-permute-done((bf16[16,512]{1,0:T(8,128)(2,1)S(1)}, bf16[16,512]{1,0:T(8,128)(2,1)S(1)}, u32[]{:S(2)}, u32[]{:S(2)}) %collective-permute-start.3) | collective-permute-done | bytes 16416 | tf_op jit(solution)/shard_map/ppermute | solution.py:41
  24.4 3.4 %collective-permute-done.4 = bf16[16,512]{1,0:T(8,128)(2,1)S(1)} collective-permute-done((bf16[16,512]{1,0:T(8,128)(2,1)S(1)}, bf16[16,512]{1,0:T(8,128)(2,1)S(1)}, u32[]{:S(2)}, u32[]{:S(2)}) %collective-permute-start.4) | collective-permute-done | bytes 16416 | tf_op jit(solution)/shard_map/ppermute | solution.py:41
  28.5 3.4 %collective-permute-done.5 = bf16[16,512]{1,0:T(8,128)(2,1)S(1)} collective-permute-done((bf16[16,512]{1,0:T(8,128)(2,1)S(1)}, bf16[16,512]{1,0:T(8,128)(2,1)S(1)}, u32[]{:S(2)}, u32[]{:S(2)}) %collective-permute-start.5) | collective-permute-done | bytes 16416 | tf_op jit(solution)/shard_map/ppermute | solution.py:41
  32.0 4.0 %collective-permute-done.6 = bf16[16,512]{1,0:T(8,128)(2,1)S(1)} collective-permute-done((bf16[16,512]{1,0:T(8,128)(2,1)S(1)}, bf16[16,512]{1,0:T(8,128)(2,1)S(1)}, u32[]{:S(2)}, u32[]{:S(2)}) %collective-permute-start.6) | collective-permute-done | bytes 16416 | tf_op jit(solution)/shard_map/ppermute | solution.py:41
  37.6 2.1 %convolution_convert_fusion = bf16[104,4096]{1,0:T(8,128)(2,1)} fusion(bf16[104,16]{0,1:T(8,128)(2,1)S(1)} %fusion.33, f32[4096]{0:T(1024)} %param.11, f32[16]{0:T(128)S(1)} %add_rsqrt_fusion, bf16[16,8192]{1,0:T(8,128)(2,1)S(1)} %constant_dynamic-update-slice_fusion, s32[]{:T(128)S(6)} %select_n.19), kind=kOutput, calls=%fused_computation | convolution fusion | flops 14319616 | bytes 1004036 | tf_op jit(solution)/shard_map/dot_general | solution.py:59
  39.7 1.4 %reshape.33 = bf16[4,2,13,4096]{3,2,1,0:T(8,128)(2,1)S(1)} reshape(bf16[104,4096]{1,0:T(8,128)(2,1)} %convolution_convert_fusion) | data formatting | bytes 1703936 | tf_op jit(solution)/shard_map/reshape | solution.py:60
  41.1 1.8 %copy.43 = bf16[4,2,13,4096]{3,1,2,0:T(2,128)(2,1)} copy(bf16[4,2,13,4096]{3,2,1,0:T(8,128)(2,1)S(1)} %reshape.33) | data formatting | bytes 1703936 | tf_op jit(solution)/shard_map/reshape | solution.py:60
  43.0 5.6 %all-to-all-start = ((bf16[4,2,13,4096]{3,1,2,0:T(2,128)(2,1)}), bf16[4,2,13,4096]{3,1,2,0:T(2,128)(2,1)S(1)}, u32[]{:S(2)}, u32[]{:S(2)}) async-start(bf16[4,2,13,4096]{3,1,2,0:T(2,128)(2,1)} %copy.43), calls=%async_computation | async-start | bytes 1703936 | tf_op jit(solution)/shard_map/all_to_all | solution.py:61
  48.6 6.2 %copy.47 = bf16[2,128,4096]{1,0,2:T(2,128)(2,1)} copy(bf16[2,128,4096]{2,1,0:T(8,128)(2,1)} %param.16) | data formatting | bytes 4194304 | tf_op args[6]
  54.8 12.6 %all-to-all-done = bf16[4,2,13,4096]{3,1,2,0:T(2,128)(2,1)S(1)} async-done(((bf16[4,2,13,4096]{3,1,2,0:T(2,128)(2,1)}), bf16[4,2,13,4096]{3,1,2,0:T(2,128)(2,1)S(1)}, u32[]{:S(2)}, u32[]{:S(2)}) %all-to-all-start) | async-done | bytes 852000 | tf_op jit(solution)/shard_map/all_to_all | solution.py:61
  67.4 4.3 %all-to-all-start.1 = ((bf16[2,128,4096]{1,0,2:T(2,128)(2,1)}), bf16[2,128,4096]{1,0,2:T(2,128)(2,1)}, u32[]{:S(2)}, u32[]{:S(2)}) async-start(bf16[2,128,4096]{1,0,2:T(2,128)(2,1)} %copy.47), calls=%async_computation.1 | async-start | bytes 4194304 | tf_op jit(solution)/shard_map/all_to_all | solution.py:38
  71.8 1.6 %fusion.43 = f32[16,128]{1,0:T(8,128)S(1)} fusion(bf16[128,4096]{1,0:T(8,128)(2,1)} %param.17, f32[4096]{0:T(1024)S(1)} %copy-done.2, f32[16]{0:T(128)S(1)} %add_rsqrt_fusion, bf16[16,8192]{1,0:T(8,128)(2,1)S(1)} %constant_dynamic-update-slice_fusion, s32[]{:T(128)S(6)} %select_n.19), kind=kOutput, calls=%fused_computation.59 | convolution fusion | flops 17039360 | bytes 1204740 | tf_op jit(solution)/shard_map/dot_general | solution.py:68
  73.4 3.1 %convolution_convert_fusion.1 = bf16[16,4096]{1,0:T(8,128)(2,1)} fusion(bf16[128,4096]{1,0:T(8,128)(2,1)} %param.19, bf16[128,4096]{1,0:T(8,128)(2,1)} %param.18, f32[16,128]{1,0:T(8,128)S(1)} %fusion.43, f32[4096]{0:T(1024)S(1)} %copy-done.2, f32[16]{0:T(128)S(1)} %add_rsqrt_fusion, bf16[16,8192]{1,0:T(8,128)(2,1)S(1)} %constant_dynamic-update-slice_fusion, ...), kind=kOutput, calls=%fused_computation.1 | convolution fusion | flops 33894400 | bytes 2384388 | tf_op jit(solution)/shard_map/dot_general | solution.py:71
  76.6 0.8 fusion.12
  78.2 0.9 fusion.21
  79.1 22.9 %all_gather.3 = bf16[4,2,13,1024]{3,2,0,1:T(8,128)(2,1)S(1)} all-gather(bf16[4,2,13,128]{3,2,0,1:T(8,128)(2,1)S(1)} %fusion.21), channel_id=1, replica_groups=mesh['ep'=4,'tp'=8] {'tp'}, dimensions={3}, use_global_device_ids=true | all-gather | bytes 239616 | tf_op jit(solution)/shard_map/all_gather | solution.py:74
  102.2 6.2 %copy.49 = bf16[2,128,8,512]{3,1,2,0:T(8,128)(2,1)} copy(bf16[2,128,8,512]{1,0,3,2:T(2,128)(2,1)} %bitcast.6) | data formatting | bytes 4194304 | tf_op jit(solution)/shard_map/all_to_all | solution.py:38
  108.3 2.1 %fusion.9 = bf16[2,4,13,512]{3,2,1,0:T(8,128)(2,1)S(1)} fusion(bf16[2,128,8,512]{3,1,2,0:T(8,128)(2,1)} %copy.49, bf16[4,2,13,8,128]{4,3,2,0,1:T(8,128)(2,1)S(1)} %reshape.39), kind=kOutput, calls=%fused_computation.9 | convolution fusion | flops 109850624 | bytes 2416640 | tf_op jit(solution)/shard_map/secpf,epfd->secpd/dot_general | solution.py:79
  111.1 3.3 %all-to-all-start.2 = ((bf16[4,2,13,512]{3,1,2,0:T(2,128)(2,1)}), bf16[4,2,13,512]{3,1,2,0:T(2,128)(2,1)S(1)}, u32[]{:S(2)}, u32[]{:S(2)}) async-start(bf16[4,2,13,512]{3,1,2,0:T(2,128)(2,1)} %copy.51), calls=%async_computation.2 | async-start | bytes 212992 | tf_op jit(solution)/shard_map/all_to_all | solution.py:86
  114.5 6.0 %all-to-all-done.2 = bf16[4,2,13,512]{3,1,2,0:T(2,128)(2,1)S(1)} async-done(((bf16[4,2,13,512]{3,1,2,0:T(2,128)(2,1)}), bf16[4,2,13,512]{3,1,2,0:T(2,128)(2,1)S(1)}, u32[]{:S(2)}, u32[]{:S(2)}) %all-to-all-start.2) | async-done | bytes 106528 | tf_op jit(solution)/shard_map/all_to_all | solution.py:86
  120.6 1.5 %fusion.24 = bf16[16,512]{1,0:T(8,128)(2,1)} fusion(f32[16,104]{1,0:T(8,128)S(1)} %select_reduce_fusion, bf16[104,512]{1,0:T(8,128)(2,1)S(1)} %reshape.35, bf16[16,512]{1,0:T(8,128)(2,1)} %reduce-scatter.2.cloned.1.call-done), kind=kOutput, calls=%fused_computation.15 | convolution fusion | flops 10248192 | bytes 145920 | tf_op jit(solution)/shard_map/dot_general | solution.py:88
  (50 shorter events, 6.4 us)
Async XLA Ops:
  6.5 70.1 %copy-start = (bf16[2,128,4096]{2,1,0:T(8,128)(2,1)S(1)}, bf16[2,128,4096]{2,1,0:T(8,128)(2,1)}, u32[]{:S(2)}) copy-start(bf16[2,128,4096]{2,1,0:T(8,128)(2,1)} %param.14) | copy-start | bytes 6291460
  6.5 5.0 %collective-permute-start = (bf16[16,512]{1,0:T(8,128)(2,1)}, bf16[16,512]{1,0:T(8,128)(2,1)S(1)}, u32[]{:S(2)}, u32[]{:S(2)}) collective-permute-start(bf16[16,512]{1,0:T(8,128)(2,1)} %param.10), channel_id=1, source_target_pairs={{0,1},{1,2},{2,3},{3,4},{4,5},{5,6},{6,7},{7,0},{8,9},{9,10},{10,1... | collective-permute-start | bytes 49160 | tf_op jit(solution)/shard_map/ppermute | solution.py:41
  11.5 4.1 %collective-permute-start.1 = (bf16[16,512]{1,0:T(8,128)(2,1)S(1)}, bf16[16,512]{1,0:T(8,128)(2,1)S(1)}, u32[]{:S(2)}, u32[]{:S(2)}) collective-permute-start(bf16[16,512]{1,0:T(8,128)(2,1)S(1)} %collective-permute-done), channel_id=1, source_target_pairs={{0,1},{1,2},{2,3},{3,4},{4,5},{5,6},{6,7},{7,0},{8,9},{9,10},{10,1... | collective-permute-start | bytes 49160 | tf_op jit(solution)/shard_map/ppermute | solution.py:41
  15.6 4.1 %collective-permute-start.2 = (bf16[16,512]{1,0:T(8,128)(2,1)S(1)}, bf16[16,512]{1,0:T(8,128)(2,1)S(1)}, u32[]{:S(2)}, u32[]{:S(2)}) collective-permute-start(bf16[16,512]{1,0:T(8,128)(2,1)S(1)} %collective-permute-done.1), channel_id=1, source_target_pairs={{0,1},{1,2},{2,3},{3,4},{4,5},{5,6},{6,7},{7,0},{8,9},{9,10},{10,1... | collective-permute-start | bytes 49160 | tf_op jit(solution)/shard_map/ppermute | solution.py:41
  19.7 4.1 %collective-permute-start.3 = (bf16[16,512]{1,0:T(8,128)(2,1)S(1)}, bf16[16,512]{1,0:T(8,128)(2,1)S(1)}, u32[]{:S(2)}, u32[]{:S(2)}) collective-permute-start(bf16[16,512]{1,0:T(8,128)(2,1)S(1)} %collective-permute-done.2), channel_id=1, source_target_pairs={{0,1},{1,2},{2,3},{3,4},{4,5},{5,6},{6,7},{7,0},{8,9},{9,10},{10,1... | collective-permute-start | bytes 49160 | tf_op jit(solution)/shard_map/ppermute | solution.py:41
  23.7 4.1 %collective-permute-start.4 = (bf16[16,512]{1,0:T(8,128)(2,1)S(1)}, bf16[16,512]{1,0:T(8,128)(2,1)S(1)}, u32[]{:S(2)}, u32[]{:S(2)}) collective-permute-start(bf16[16,512]{1,0:T(8,128)(2,1)S(1)} %collective-permute-done.3), channel_id=1, source_target_pairs={{0,1},{1,2},{2,3},{3,4},{4,5},{5,6},{6,7},{7,0},{8,9},{9,10},{10,1... | collective-permute-start | bytes 49160 | tf_op jit(solution)/shard_map/ppermute | solution.py:41
  27.8 4.1 %collective-permute-start.5 = (bf16[16,512]{1,0:T(8,128)(2,1)S(1)}, bf16[16,512]{1,0:T(8,128)(2,1)S(1)}, u32[]{:S(2)}, u32[]{:S(2)}) collective-permute-start(bf16[16,512]{1,0:T(8,128)(2,1)S(1)} %collective-permute-done.4), channel_id=1, source_target_pairs={{0,1},{1,2},{2,3},{3,4},{4,5},{5,6},{6,7},{7,0},{8,9},{9,10},{10,1... | collective-permute-start | bytes 49160 | tf_op jit(solution)/shard_map/ppermute | solution.py:41
  31.9 4.1 %collective-permute-start.6 = (bf16[16,512]{1,0:T(8,128)(2,1)S(1)}, bf16[16,512]{1,0:T(8,128)(2,1)S(1)}, u32[]{:S(2)}, u32[]{:S(2)}) collective-permute-start(bf16[16,512]{1,0:T(8,128)(2,1)S(1)} %collective-permute-done.5), channel_id=1, source_target_pairs={{0,1},{1,2},{2,3},{3,4},{4,5},{5,6},{6,7},{7,0},{8,9},{9,10},{10,1... | collective-permute-start | bytes 49160 | tf_op jit(solution)/shard_map/ppermute | solution.py:41
  43.0 24.4 %all-to-all-start = ((bf16[4,2,13,4096]{3,1,2,0:T(2,128)(2,1)}), bf16[4,2,13,4096]{3,1,2,0:T(2,128)(2,1)S(1)}, u32[]{:S(2)}, u32[]{:S(2)}) async-start(bf16[4,2,13,4096]{3,1,2,0:T(2,128)(2,1)} %copy.43), calls=%async_computation | async-start | bytes 1703936 | tf_op jit(solution)/shard_map/all_to_all | solution.py:61
  54.8 17.0 %copy-start.2 = (f32[4096]{0:T(1024)S(1)}, f32[4096]{0:T(1024)}, u32[]{:S(2)}) copy-start(f32[4096]{0:T(1024)} %param.11) | copy-start | bytes 49156
  67.4 34.8 %all-to-all-start.1 = ((bf16[2,128,4096]{1,0,2:T(2,128)(2,1)}), bf16[2,128,4096]{1,0,2:T(2,128)(2,1)}, u32[]{:S(2)}, u32[]{:S(2)}) async-start(bf16[2,128,4096]{1,0,2:T(2,128)(2,1)} %copy.47), calls=%async_computation.1 | async-start | bytes 4194304 | tf_op jit(solution)/shard_map/all_to_all | solution.py:38
  71.7 48.9 %reduce-scatter.2.cloned.1.call-start = ((), (), s32[]{:S(2)}) async-start(), calls=%async_computation.4 | async-start | bytes 147456 | tf_op jit(solution)/shard_map/reduce_scatter | solution.py:83
  76.6 1.6 %copy-start.1 = (bf16[2,128,4096]{2,1,0:T(8,128)(2,1)S(1)}, bf16[2,128,4096]{2,1,0:T(8,128)(2,1)}, u32[]{:S(2)}) copy-start(bf16[2,128,4096]{2,1,0:T(8,128)(2,1)} %param.15) | copy-start | bytes 6291460
  108.3 6.1 %copy-start.3 = (f32[16,4]{0,1:T(4,128)S(1)}, f32[16,4]{0,1:T(4,128)}, u32[]{:S(2)}) copy-start(f32[16,4]{0,1:T(4,128)} %param.13) | copy-start | bytes 772
  111.1 9.4 %all-to-all-start.2 = ((bf16[4,2,13,512]{3,1,2,0:T(2,128)(2,1)}), bf16[4,2,13,512]{3,1,2,0:T(2,128)(2,1)S(1)}, u32[]{:S(2)}, u32[]{:S(2)}) async-start(bf16[4,2,13,512]{3,1,2,0:T(2,128)(2,1)} %copy.51), calls=%async_computation.2 | async-start | bytes 212992 | tf_op jit(solution)/shard_map/all_to_all | solution.py:86
Sparse Core Ops, SparseCore 0:
  76.7 33.0 reduce-scatter.1
